TPU v7x, 32 devices: a whole 2x2x4 slice. The times are simulated.
32 devices in a mesh: sp: 4 (over z), tp: 2 (over y), dp: 4 (over x, core).
Axes of the slice: x: 2, y: 2, z: 4, core: 2. Of those that a mesh axis runs over, the one named last changes fastest.
Arguments:
- latent: bfloat16 [5120, 3072], P(('dp', 'sp', 'tp')), parts along dimension 0, may hold values from -6 to 6
- condition: float32 [12288], P('dp'), parts along dimension 0, may hold values from -8 to 8
- ctx_condition: float32 [3072], replicated, may hold values from -8 to 8
- context: bfloat16 [512, 3072], P(('dp', 'sp')), parts along dimension 0, may hold values from -6 to 6
- mod_shift: bfloat16 [3072, 3072], P('sp', 'tp'), may hold values from -0.109375 to 0.109375
- mod_scale: bfloat16 [3072, 3072], P('sp', 'tp'), may hold values from -0.109375 to 0.109375
- mod_gate: bfloat16 [3072, 3072], P('sp', 'tp'), may hold values from -0.109375 to 0.109375
- norm_gain: float32 [3072], replicated, may hold values from 0.5 to 6
- w_query: bfloat16 [3072, 3072], P(None, 'tp'), may hold values from -0.109375 to 0.109375
- key_weight: bfloat16 [3072, 512], P(None, 'tp'), may hold values from -0.109375 to 0.109375
- value_weight: bfloat16 [3072, 512], P(None, 'tp'), may hold values from -0.109375 to 0.109375
- w_gate: bfloat16 [3072, 3072], P(None, 'tp'), may hold values from -0.109375 to 0.109375
- w_out: bfloat16 [3072, 3072], P('tp'), may hold values from -1.5 to 1.5
- sink_logit: float32 [48], P('tp'), may hold values from 4 to 7.5
Outputs:
- updated_latent: bfloat16 [5120, 3072], P(('dp', 'sp', 'tp')), parts along dimension 0
There are 4 independent parts, one for each index of `dp`. A program takes and returns all parts, laid end to end along the dimension named above; an argument that names none is the same for every part. Nothing has to cross between parts.
All inputs are finite; a program needn't handle non-finite values.
Results may differ from a plain program's by a relative error of at most 0.02.
The roundings to bfloat16 on the way count: a program that leaves them out, or rounds other values in their place, can miss the bound.
Values may be sent and summed in bfloat16 or wider, within the bound.
A program may use at most 128 MiB of HBM per device.

v0:
```python
import math
import jax
import jax.numpy as jnp
from jax import lax
from jax.sharding import PartitionSpec as P

HEAD_SIZE = 64
WINDOW = 128
GRID_W = 64
NORM_EPS = 1e-06
MASK_VALUE = -1e30


def with_halo(block, sides, width):
    for axis, dim in sides:
        count = lax.axis_size(axis)
        forward = [(i, i + 1) for i in range(count - 1)]
        backward = [(target, source) for source, target in forward]
        low = lax.ppermute(
            lax.slice_in_dim(block, block.shape[dim] - width, None, axis=dim), axis, forward
        )
        high = lax.ppermute(lax.slice_in_dim(block, 0, width, axis=dim), axis, backward)
        block = jnp.concatenate([low, block, high], axis=dim)
    return block


def modulate(row_data, gain_vec, shift_vec, scale_vec):
    values = row_data.astype(jnp.float32)
    inverse = lax.rsqrt(jnp.mean(values * values, axis=-1, keepdims=True) + NORM_EPS)
    return (values * inverse * gain_vec * (1.0 + scale_vec) + shift_vec).astype(jnp.bfloat16)


def rotate(projected, positions):
    row_count = projected.shape[0]
    head_count = projected.shape[1] // HEAD_SIZE
    quarter = HEAD_SIZE // 4
    half_dim = HEAD_SIZE // 2
    inverse = jnp.exp(-math.log(10000.0) * jnp.arange(quarter, dtype=jnp.float32) / quarter)
    grid_row = (positions // GRID_W).astype(jnp.float32)
    mesh_column = (positions % GRID_W).astype(jnp.float32)
    angles = jnp.concatenate([grid_row[:, None] * inverse, mesh_column[:, None] * inverse], axis=1)
    cosine = jnp.cos(angles)[:, None, :]
    sine_table = jnp.sin(angles)[:, None, :]
    shaped = projected.reshape(row_count, head_count, HEAD_SIZE)
    first_half = shaped[..., :half_dim]
    second = shaped[..., half_dim:]
    turned = jnp.concatenate(
        [first_half * cosine - second * sine_table, second * cosine + first_half * sine_table],
        axis=-1,
    )
    return turned.reshape(row_count, head_count * HEAD_SIZE)


def attend(
    queries, key_rows, value_rows, ctx_keys, ctx_values, sink_logit, q_begin, k_begin, seq_total
):
    row_count = queries.shape[0]
    key_count = key_rows.shape[0]
    ctx_count = ctx_keys.shape[0]
    kv_heads = key_rows.shape[1] // HEAD_SIZE
    head_count = queries.shape[1] // HEAD_SIZE
    group_size = head_count // kv_heads
    factor = 1.0 / math.sqrt(HEAD_SIZE)
    q_heads = queries.reshape(row_count, kv_heads, group_size, HEAD_SIZE)
    k_heads = key_rows.reshape(key_count, kv_heads, HEAD_SIZE)
    v_heads = value_rows.reshape(key_count, kv_heads, HEAD_SIZE)
    ck_heads = ctx_keys.reshape(ctx_count, kv_heads, HEAD_SIZE)
    cv_heads = ctx_values.reshape(ctx_count, kv_heads, HEAD_SIZE)
    near_scores = (
        jnp.einsum("qkgd,skd->kgqs", q_heads, k_heads, preferred_element_type=jnp.float32) * factor
    )
    q_pos = q_begin + jnp.arange(row_count, dtype=jnp.int32)
    k_pos = k_begin + jnp.arange(key_count, dtype=jnp.int32)
    in_window = (jnp.abs(q_pos[:, None] - k_pos[None, :]) <= WINDOW) & (
        (k_pos >= 0) & (k_pos < seq_total)
    )[None, :]
    near_scores = jnp.where(in_window, near_scores, MASK_VALUE)
    ctx_scores = (
        jnp.einsum("qkgd,skd->kgqs", q_heads, ck_heads, preferred_element_type=jnp.float32) * factor
    )
    sink_score = sink_logit.reshape(kv_heads, group_size)[:, :, None, None]
    peak_score = jnp.maximum(
        jnp.maximum(
            jnp.max(near_scores, axis=-1, keepdims=True),
            jnp.max(ctx_scores, axis=-1, keepdims=True),
        ),
        sink_score,
    )
    near_exp = jnp.exp(near_scores - peak_score)
    ctx_exp = jnp.exp(ctx_scores - peak_score)
    softmax_denominator = (
        jnp.sum(near_exp, axis=-1, keepdims=True)
        + jnp.sum(ctx_exp, axis=-1, keepdims=True)
        + jnp.exp(sink_score - peak_score)
    )
    near_weights = (near_exp / softmax_denominator).astype(jnp.bfloat16)
    ctx_weights = (ctx_exp / softmax_denominator).astype(jnp.bfloat16)
    result = jnp.einsum("kgqs,skd->qkgd", near_weights, v_heads, preferred_element_type=jnp.float32)
    result = result + jnp.einsum(
        "kgqs,skd->qkgd", ctx_weights, cv_heads, preferred_element_type=jnp.float32
    )
    return result.reshape(row_count, head_count * HEAD_SIZE)


def shards(
    latent,
    condition,
    ctx_condition,
    context,
    mod_shift,
    mod_scale,
    mod_gate,
    norm_gain,
    w_query,
    key_weight,
    value_weight,
    w_gate,
    w_out,
    sink_logit,
):
    sp_count = lax.axis_size("sp")
    sp_rank = lax.axis_index("sp")
    mod_rows = mod_shift.shape[0]
    cond_act = jax.nn.silu(condition).astype(jnp.bfloat16)
    ctx_act = jax.nn.silu(ctx_condition).astype(jnp.bfloat16)
    first_row = sp_rank * mod_rows
    lat_piece = lax.dynamic_slice_in_dim(cond_act, first_row, mod_rows, 0)
    ctx_piece = lax.dynamic_slice_in_dim(ctx_act, first_row, mod_rows, 0)
    both_conds = jnp.stack([lat_piece, ctx_piece])
    partial_value = jnp.concatenate(
        [
            jnp.dot(both_conds, mod_shift, preferred_element_type=jnp.float32),
            jnp.dot(both_conds, mod_scale, preferred_element_type=jnp.float32),
            jnp.dot(lat_piece[None, :], mod_gate, preferred_element_type=jnp.float32),
        ],
        axis=0,
    )
    summed = lax.psum(partial_value, "sp")
    vectors = lax.all_gather(summed, "tp", axis=1, tiled=True)
    lat_shift = vectors[0]
    ctx_shift = vectors[1]
    lat_scale = vectors[2]
    ctx_scale = vectors[3]
    lat_gate = vectors[4]
    hidden = modulate(latent, norm_gain, lat_shift, lat_scale)
    ctx_hidden = modulate(context, norm_gain, ctx_shift, ctx_scale)
    kv_width = key_weight.shape[1]
    q_width = w_query.shape[1]
    ctx_pair = jnp.concatenate(
        [
            jnp.dot(ctx_hidden, key_weight, preferred_element_type=jnp.float32).astype(
                jnp.bfloat16
            ),
            jnp.dot(ctx_hidden, value_weight, preferred_element_type=jnp.float32).astype(
                jnp.bfloat16
            ),
        ],
        axis=1,
    )
    ctx_all = lax.all_gather(ctx_pair, "sp", axis=0, tiled=True)
    row_piece = lax.all_gather(hidden, "tp", axis=0, tiled=True)
    projected = jnp.concatenate(
        [
            jnp.dot(row_piece, w_query, preferred_element_type=jnp.float32),
            jnp.dot(row_piece, key_weight, preferred_element_type=jnp.float32),
            jnp.dot(row_piece, value_weight, preferred_element_type=jnp.float32),
            jnp.dot(row_piece, w_gate, preferred_element_type=jnp.float32),
        ],
        axis=1,
    )
    block_rows = projected.shape[0]
    q_begin = sp_rank * block_rows
    positions = q_begin + jnp.arange(block_rows, dtype=jnp.int32)
    queries = rotate(projected[:, :q_width], positions).astype(jnp.bfloat16)
    key_rows = rotate(projected[:, q_width : q_width + kv_width], positions).astype(jnp.bfloat16)
    value_rows = projected[:, q_width + kv_width : q_width + 2 * kv_width].astype(jnp.bfloat16)
    gate_proj = projected[:, q_width + 2 * kv_width :].astype(jnp.bfloat16)
    key_value = jnp.concatenate([key_rows, value_rows], axis=1)
    padded = with_halo(key_value, (("sp", 0),), WINDOW)
    attended = attend(
        queries,
        padded[:, :kv_width],
        padded[:, kv_width:],
        ctx_all[:, :kv_width],
        ctx_all[:, kv_width:],
        sink_logit,
        q_begin,
        q_begin - WINDOW,
        block_rows * sp_count,
    )
    mixed = (attended * jax.nn.silu(gate_proj.astype(jnp.float32))).astype(jnp.bfloat16)
    branch = lax.psum_scatter(
        jnp.dot(mixed, w_out, preferred_element_type=jnp.float32).astype(jnp.bfloat16),
        "tp",
        scatter_dimension=0,
        tiled=True,
    ).astype(jnp.float32)
    return (latent.astype(jnp.float32) + lat_gate * branch).astype(jnp.bfloat16)


def solution(mesh):
    return jax.shard_map(
        shards,
        mesh=mesh,
        in_specs=(
            P(("dp", "sp", "tp"), None),
            P("dp"),
            P(),
            P(("dp", "sp"), None),
            P("sp", "tp"),
            P("sp", "tp"),
            P("sp", "tp"),
            P(),
            P(None, "tp"),
            P(None, "tp"),
            P(None, "tp"),
            P(None, "tp"),
            P("tp", None),
            P("tp"),
        ),
        out_specs=P(("dp", "sp", "tp"), None),
        check_vma=False,
    )
```

profile of v0, /device:TPU:0, one launch (start us, length us, event | category | flops | bytes accessed | tf_op | source)
XLA Modules:
  0.0 179.3 jit_solution(17299851433781400490)
XLA Ops:
  6.5 0.0 copy-start
  6.5 0.0 all-gather.2.cloned.1.call-start
  6.5 0.9 multiply_convert_fusion.1
  7.5 0.7 copy-done
  8.2 0.4 fusion.30
  8.6 0.3 copy-done.5
  8.9 0.4 fusion.31
  9.3 0.7 copy-done.6
  10.1 0.4 fusion.37
  10.5 21.4 %psum.7 = f32[5,1536]{1,0:T(8,128)S(1)} all-reduce(f32[5,1536]{1,0:T(8,128)S(1)} %pad_maximum_fusion.5), channel_id=1, replica_groups=mesh['sp'=4,'tp'=2,'dp'=4] {'sp'}, use_global_device_ids=true, to_apply=%region_0.1 | all-reduce | flops 7680 | bytes 61440 | tf_op jit(solution)/shard_map/psum | solution.py:138
  31.9 4.8 %all_gather.9 = f32[5,3072]{1,0:T(8,128)S(1)} all-gather(f32[5,1536]{1,0:T(8,128)S(1)} %psum.7), channel_id=1, replica_groups=mesh['sp'=4,'tp'=2,'dp'=4] {'tp'}, dimensions={1}, use_global_device_ids=true | all-gather | bytes 92160 | tf_op jit(solution)/shard_map/all_gather | solution.py:139
  36.7 0.1 fusion.36
  36.7 0.0 copy-done.4
  36.7 0.3 fusion.6
  37.0 0.0 copy-done.9
  37.0 1.4 fusion.10
  38.4 0.0 all-gather.2.cloned.1.call-update
  38.4 0.0 copy-start.10
  38.4 0.0 reduce-scatter.2.cloned.1.call-start
  38.5 0.0 copy-done.7
  38.5 0.2 fusion.15
  38.7 0.0 copy-done.8
  38.7 0.4 convolution_convert_fusion.4
  39.1 1.8 %convolution_convert_fusion.3 = bf16[32,256]{1,0:T(8,128)(2,1)S(1)} fusion(bf16[3072,256]{1,0:T(8,128)(2,1)} %param.24, bf16[32,3072]{1,0:T(8,128)(2,1)S(1)} %copy-done.7, f32[3072]{0:T(1024)S(1)} %bitcast.93, f32[3072]{0:T(1024)S(1)} %bitcast.95, f32[3072]{0:T(1024)S(1)} %copy-done.9, f32[32]{0:T(128)S(1)} %add_rsqrt_fusion.1), kind=kOutput, calls=%fused_computation.30 | convolution fusion | flops 50929664 | bytes 1822848 | tf_op jit(solution)/shard_map/dot_general | solution.py:154
  41.0 13.4 %all_gather.11 = bf16[128,512]{1,0:T(8,128)(2,1)S(1)} all-gather(bf16[32,512]{1,0:T(8,128)(2,1)S(1)} %pad_maximum_fusion.7), channel_id=1, replica_groups=mesh['sp'=4,'tp'=2,'dp'=4] {'sp'}, dimensions={0}, use_global_device_ids=true | all-gather | bytes 163840 | tf_op jit(solution)/shard_map/all_gather | solution.py:160
  54.3 0.1 copy.26
  54.4 0.0 copy-done.10
  54.5 0.1 max.30
  54.5 0.1 copy.27
  54.7 0.1 broadcast_multiply_fusion.1
  54.8 0.2 fusion.21
  55.0 0.3 fusion.14
  55.3 13.1 %all-gather.2.cloned.1.call-done = bf16[320,3072]{1,0:T(8,128)(2,1)} async-done(((bf16[160,3072]{1,0:T(8,128)(2,1)}), bf16[320,3072]{1,0:T(8,128)(2,1)}) %all-gather.2.cloned.1.call-update) | async-done | bytes 1966096 | tf_op jit(solution)/shard_map/all_gather | solution.py:161
  68.4 2.6 %fusion.38 = f32[320,256]{0,1:T(8,128)S(1)} fusion(bf16[320,3072]{1,0:T(8,128)(2,1)} %all-gather.2.cloned.1.call-done, bf16[3072,256]{1,0:T(8,128)(2,1)S(1)} %copy-done.8), kind=kOutput, calls=%fused_computation.87 | convolution fusion | flops 503316480 | bytes 3866624 | tf_op jit(solution)/shard_map/dot_general | solution.py:165
  71.0 0.1 subtract_convert_fusion.1
  71.1 0.1 copy.22
  71.3 0.0 copy-start.11
  71.3 2.8 %convolution_convert_fusion.2 = bf16[320,256]{1,0:T(8,128)(2,1)S(1)} fusion(bf16[320,3072]{1,0:T(8,128)(2,1)} %all-gather.2.cloned.1.call-done, bf16[3072,256]{1,0:T(8,128)(2,1)} %param.24), kind=kOutput, calls=%fused_computation.29 | convolution fusion | flops 503398400 | bytes 3702784 | tf_op jit(solution)/shard_map/dot_general | solution.py:166
  74.1 3.4 %collective-permute-start = (bf16[128,512]{1,0:T(8,128)(2,1)S(1)}, bf16[128,512]{1,0:T(8,128)(2,1)S(1)}, u32[]{:S(2)}, u32[]{:S(2)}) collective-permute-start(bf16[128,512]{1,0:T(8,128)(2,1)S(1)} %get-tuple-element.11), channel_id=1, source_target_pairs={{0,8},{8,16},{16,24},{1,9},{9,17},{17,25},{2,10},{10,18},{18,26},{... | collective-permute-start | bytes 393224 | tf_op jit(solution)/shard_map/ppermute | solution.py:19
  77.5 1.5 collective-permute-start.1
  79.0 0.0 copy-done.11
  79.0 7.7 %fusion.39 = f32[320,1536]{0,1:T(8,128)S(1)} fusion(bf16[320,3072]{1,0:T(8,128)(2,1)S(1)} %copy-done.11, bf16[3072,1536]{1,0:T(8,128)(2,1)} %param.22), kind=kOutput, calls=%fused_computation.88 | convolution fusion | flops 3019898880 | bytes 13369344 | tf_op jit(solution)/shard_map/dot_general | solution.py:164
  86.8 0.4 subtract_convert_fusion
  87.1 0.2 pad_maximum_fusion
  87.3 2.8 %bitcast_reduce_fusion = (f32[4,6,320]{2,1,0:T(8,128)S(1)}, f32[4,128,320,6]{1,2,3,0:T(8,128)}) fusion(bf16[128,4,64,1]{0,2,3,1:T(8,128)(2,1)S(1)} %bitcast.91, bf16[320,4,6,64]{0,3,2,1:T(8,128)(2,1)S(1)} %bitcast.83), kind=kOutput, calls=%fused_computation.8 | convolution fusion | flops 127787520 | bytes 5011456 | tf_op jit(solution)/shard_map/qkgd,skd->kgqs/dot_general | solution.py:79
  90.1 0.0 collective-permute-done
  90.1 0.0 collective-permute-done.1
  90.1 0.8 fusion.34
  90.9 1.2 copy.24
  92.1 0.0 copy-start.3
  92.1 4.5 %fusion.1 = (f32[4,6,320]{2,1,0:T(8,128)S(1)}, f32[4,576,320,6]{1,2,3,0:T(8,128)S(1)}) fusion(pred[320,576]{1,0:T(8,128)(4,1)S(1)} %fusion.14, bf16[576,4,64,1]{0,2,3,1:T(8,128)(2,1)S(1)} %bitcast.87, bf16[320,4,6,64]{0,3,2,1:T(8,128)(2,1)S(1)} %bitcast.84), kind=kOutput, calls=%fused_computation.4 | convolution fusion | flops 579494400 | bytes 19187712 | tf_op jit(solution)/shard_map/qkgd,skd->kgqs/dot_general | solution.py:70
  96.6 0.1 maximum_maximum_fusion
  96.7 2.6 %fusion.4 = f32[4,6,320]{2,1,0:T(8,128)S(1)} fusion(f32[4,128,320,6]{1,2,3,0:T(8,128)S(1)} %copy-done.3, f32[4,6,320]{2,1,0:T(8,128)S(1)} %maximum_maximum_fusion), kind=kLoop, calls=%fused_computation.11 | loop fusion | flops 2941440 | bytes 3993600 | tf_op jit(solution)/shard_map/reduce_sum | solution.py:93
  99.3 5.5 %fusion = f32[4,6,320]{2,1,0:T(8,128)S(1)} fusion(f32[4,576,320,6]{1,2,3,0:T(8,128)S(1)} %get-tuple-element.25, f32[4,6,320]{2,1,0:T(8,128)S(1)} %maximum_maximum_fusion, pred[320,576]{1,0:T(8,128)(4,1)S(1)} %fusion.14), kind=kLoop, calls=%fused_computation.3 | loop fusion | flops 17687040 | bytes 17940480 | tf_op jit(solution)/shard_map/reduce_sum | solution.py:92
  104.7 0.0 copy-done.2
  104.7 0.2 copy.23
  104.9 0.1 exponential_add_fusion
  105.0 5.7 %fusion.12 = f32[4,64,6,320]{3,1,2,0:T(8,128)S(1)} fusion(bf16[128,4,64,1]{0,2,3,1:T(8,128)(2,1)S(1)} %bitcast.96, f32[4,128,320,6]{1,2,3,0:T(8,128)} %get-tuple-element.27, f32[4,6,320]{2,1,0:T(8,128)S(1)} %exponential_add_fusion, f32[4,6,320]{2,1,0:T(8,128)S(1)} %maximum_maximum_fusion), kind=kOutput, calls=%fused_computation.24 | convolution fusion | flops 129761280 | bytes 6025216 | tf_op jit(solution)/shard_map/kgqs,skd->qkgd/dot_general | solution.py:99
  110.7 10.9 %fusion.13 = f32[4,64,6,320]{3,1,2,0:T(8,128)} fusion(f32[4,64,6,320]{3,1,2,0:T(8,128)S(1)} %fusion.12, bf16[576,4,64,1]{0,2,3,1:T(8,128)(2,1)S(1)} %bitcast.90, f32[4,576,320,6]{1,2,3,0:T(8,128)} %copy-done.2, f32[4,6,320]{2,1,0:T(8,128)S(1)} %exponential_add_fusion, f32[4,6,320]{2,1,0:T(8,128)S(1)} %maximum_maximum_fusion, pred[320,576]{1,0:T(8,128)(4,1)S(1)} %fusion.14), kind=kOutput, calls=%fused_computation.25 | convolution fusion | flops 588840960 | bytes 22167552 | tf_op jit(solution)/shard_map/kgqs,skd->qkgd/dot_general | solution.py:98
  121.6 2.0 %copy.28 = f32[320,1536]{1,0:T(8,128)S(1)} copy(f32[320,1536]{0,1:T(8,128)} %bitcast.85) | data formatting | bytes 3932160 | tf_op jit(solution)/shard_map/reshape | solution.py:102
  123.6 14.5 %convolution_convert_fusion = bf16[320,3072]{1,0:T(8,128)(2,1)} fusion(bf16[1536,3072]{1,0:T(8,128)(2,1)} %param.26, f32[320,1536]{1,0:T(8,128)S(1)} %copy.28, bf16[320,3072]{1,0:T(8,128)(2,1)} %all-gather.2.cloned.1.call-done, bf16[3072,1536]{1,0:T(8,128)(2,1)} %param.25), kind=kOutput, calls=%fused_computation.6 | convolution fusion | flops 6044712960 | bytes 24772608 | tf_op jit(solution)/shard_map/dot_general | solution.py:193
  138.2 0.0 reduce-scatter.2.cloned.1.call-update
  138.2 31.8 %reduce-scatter.2.cloned.1.call-done = bf16[160,3072]{1,0:T(8,128)(2,1)} async-done(((bf16[320,3072]{1,0:T(8,128)(2,1)}), bf16[160,3072]{1,0:T(8,128)(2,1)}) %reduce-scatter.2.cloned.1.call-update) | async-done | bytes 983056 | tf_op jit(solution)/shard_map/reduce_scatter | solution.py:192
  170.0 2.5 %fusion.11 = bf16[160,3072]{1,0:T(8,128)(2,1)} fusion(bf16[160,3072]{1,0:T(8,128)(2,1)S(1)} %copy-done.4, bf16[160,3072]{1,0:T(8,128)(2,1)} %reduce-scatter.2.cloned.1.call-done, f32[3072]{0:T(1024)S(1)} %bitcast.97), kind=kLoop, calls=%fused_computation.22 | loop fusion | flops 2457600 | bytes 2961408 | tf_op jit(solution)/shard_map/convert_element_type | solution.py:198
  (26 shorter events, 0.2 us)
Async XLA Ops:
  6.5 1.7 copy-start
  6.5 61.9 %all-gather.2.cloned.1.call-start = ((), (), s32[]{:S(2)}) async-start(), calls=%async_computation.1 | async-start | bytes 2949120 | tf_op jit(solution)/shard_map/all_gather | solution.py:161
  6.5 2.4 %copy-start.5 = (bf16[768,1536]{1,0:T(8,128)(2,1)S(1)}, bf16[768,1536]{1,0:T(8,128)(2,1)}, u32[]{:S(2)}) copy-start(bf16[768,1536]{1,0:T(8,128)(2,1)} %param.18) | copy-start | bytes 7077892
  8.2 1.8 %copy-start.6 = (bf16[768,1536]{1,0:T(8,128)(2,1)S(1)}, bf16[768,1536]{1,0:T(8,128)(2,1)}, u32[]{:S(2)}) copy-start(bf16[768,1536]{1,0:T(8,128)(2,1)} %param.20) | copy-start | bytes 7077892
  8.9 27.8 %copy-start.4 = (bf16[160,3072]{1,0:T(8,128)(2,1)S(1)}, bf16[160,3072]{1,0:T(8,128)(2,1)}, u32[]{:S(2)}) copy-start(bf16[160,3072]{1,0:T(8,128)(2,1)} %param.14) | copy-start | bytes 2949124
  10.1 27.0 %copy-start.9 = (f32[3072]{0:T(1024)S(1)}, f32[3072]{0:T(1024)}, u32[]{:S(2)}) copy-start(f32[3072]{0:T(1024)} %param.21) | copy-start | bytes 36868
  10.5 28.0 %copy-start.7 = (bf16[32,3072]{1,0:T(8,128)(2,1)S(1)}, bf16[32,3072]{1,0:T(8,128)(2,1)}, u32[]{:S(2)}) copy-start(bf16[32,3072]{1,0:T(8,128)(2,1)} %param.17) | copy-start | bytes 589828
  10.5 28.2 %copy-start.8 = (bf16[3072,256]{1,0:T(8,128)(2,1)S(1)}, bf16[3072,256]{1,0:T(8,128)(2,1)}, u32[]{:S(2)}) copy-start(bf16[3072,256]{1,0:T(8,128)(2,1)} %param.23) | copy-start | bytes 4718596
  38.4 16.0 %copy-start.10 = (f32[24]{0:T(128)S(1)}, f32[24]{0:T(128)}, u32[]{:S(2)}) copy-start(f32[24]{0:T(128)} %param.27) | copy-start | bytes 292
  38.4 131.5 %reduce-scatter.2.cloned.1.call-start = ((), (), s32[]{:S(2)}) async-start(), calls=%async_computation.2 | async-start | bytes 2949120 | tf_op jit(solution)/shard_map/reduce_scatter | solution.py:192
  71.3 7.7 %copy-start.11 = (bf16[320,3072]{1,0:T(8,128)(2,1)S(1)}, bf16[320,3072]{1,0:T(8,128)(2,1)}, u32[]{:S(2)}) copy-start(bf16[320,3072]{1,0:T(8,128)(2,1)} %all-gather.2.cloned.1.call-done) | copy-start | bytes 5898244
  74.1 16.0 %collective-permute-start = (bf16[128,512]{1,0:T(8,128)(2,1)S(1)}, bf16[128,512]{1,0:T(8,128)(2,1)S(1)}, u32[]{:S(2)}, u32[]{:S(2)}) collective-permute-start(bf16[128,512]{1,0:T(8,128)(2,1)S(1)} %get-tuple-element.11), channel_id=1, source_target_pairs={{0,8},{8,16},{16,24},{1,9},{9,17},{17,25},{2,10},{10,18},{18,26},{... | collective-permute-start | bytes 393224 | tf_op jit(solution)/shard_map/ppermute | solution.py:19
  77.5 12.6 %collective-permute-start.1 = (bf16[128,512]{1,0:T(8,128)(2,1)S(1)}, bf16[128,512]{1,0:T(8,128)(2,1)S(1)}, u32[]{:S(2)}, u32[]{:S(2)}) collective-permute-start(bf16[128,512]{1,0:T(8,128)(2,1)S(1)} %get-tuple-element.12), channel_id=1, source_target_pairs={{8,0},{16,8},{24,16},{9,1},{17,9},{25,17},{10,2},{18,10},{26,18},{... | collective-permute-start | bytes 393224 | tf_op jit(solution)/shard_map/ppermute | solution.py:22
  92.1 4.6 %copy-start.3 = (f32[4,128,320,6]{1,2,3,0:T(8,128)S(1)}, f32[4,128,320,6]{1,2,3,0:T(8,128)}, u32[]{:S(2)}) copy-start(f32[4,128,320,6]{1,2,3,0:T(8,128)} %get-tuple-element.27) | copy-start | bytes 11796484
  96.6 8.1 %copy-start.2 = (f32[4,576,320,6]{1,2,3,0:T(8,128)}, f32[4,576,320,6]{1,2,3,0:T(8,128)S(1)}, u32[]{:S(2)}) copy-start(f32[4,576,320,6]{1,2,3,0:T(8,128)S(1)} %get-tuple-element.25) | copy-start | bytes 53084164
  138.2 34.3 %copy-start.1 = (bf16[768,1536]{1,0:T(8,128)(2,1)S(1)}, bf16[768,1536]{1,0:T(8,128)(2,1)}, u32[]{:S(2)}) copy-start(bf16[768,1536]{1,0:T(8,128)(2,1)} %param.19) | copy-start | bytes 7077892
Sparse Core Ops, SparseCore 0:
  38.6 29.8 all-gather.1
  138.3 31.6 reduce-scatter.1
where the time goes:
time: 180 us; the launch traced here: 179 us
  matrix products  55 us (31%)
  waiting for transfers between devices  44.9 us (25%)
  blocking collectives  39.5 us (22%)
  other arithmetic  14.8 us (8%)
  between operations  13.7 us (8%)
  local copies, waits for them, and re-layouts  6.34 us (4%)
  starting transfers between devices  4.91 us (3%)
    reduce_scatter x1, waiting for transfers between devices, shards(): lax.psum_scatter(jnp.dot(mixed, w_out, preferred_element_type=jnp.float32...  31.8 us
    psum x1, blocking collectives, shards(): summed = lax.psum(partial_value, 'sp')  21.4 us
    dot_general x1, matrix products, shards(): jnp.dot(mixed, w_out, preferred_element_type=jnp.float32)  14.5 us
    all_gather x1, blocking collectives, shards(): ctx_all = lax.all_gather(ctx_pair, 'sp', axis=0, tiled=True)  13.4 us
    all_gather x1, waiting for transfers between devices, shards(): row_piece = lax.all_gather(hidden, 'tp', axis=0, tiled=True)  13.1 us
    dot_general x1, matrix products, attend(): jnp.einsum('kgqs,skd->qkgd', near_weights, v_heads, preferred_element_typ...  10.9 us
    dot_general x1, matrix products, shards(): jnp.dot(row_piece, w_query, preferred_element_type=jnp.float32)  7.75 us
    dot_general x1, matrix products, attend(): jnp.einsum('kgqs,skd->qkgd', ctx_weights, cv_heads, preferred_element_typ...  5.69 us
  transfers between devices with their start and end apart: 4, of which 2 were waited for; matrix products, arithmetic and copies ran while one was open for 8% of the time, Pallas kernels for 0%

commit v1 on v0

--- a/solution.py
+++ b/solution.py
@@ -135,7 +135,21 @@
         ],
         axis=0,
     )
-    summed = lax.psum(partial_value, "sp")
+
+    def group_show(slab_in, group_axis="sp"):
+        count_all = lax.axis_size(group_axis)
+
+        def perform_modes(spare, moved):
+            if moved >= count_all:
+                return spare
+            by_rank = []
+            for j in range(count_all):
+                by_rank.append((j, j ^ moved))
+            return perform_modes(spare + lax.ppermute(spare, group_axis, perm=by_rank), 2 * moved)
+
+        return perform_modes(slab_in, 1)
+
+    summed = group_show(partial_value)
     vectors = lax.all_gather(summed, "tp", axis=1, tiled=True)
     lat_shift = vectors[0]
     ctx_shift = vectors[1]

time: 180 us -> 172 us (0.956)
  blocking collectives: 39.5 us -> 19.1 us
  waiting for transfers between devices: 44.9 us -> 52.2 us
  starting transfers between devices: 4.91 us -> 11.1 us
    psum x1 -> x0, blocking collectives: 21.4 us -> none  [shards(): summed = lax.psum(partial_value, 'sp')]
    ppermute x0 -> x2, starting transfers between devices: none -> 6.22 us  [perform_modes(): lax.ppermute(spare, group_axis, perm=by_rank)]
    ppermute x0 -> x2, waiting for transfers between devices: none -> 3.81 us  [perform_modes(): lax.ppermute(spare, group_axis, perm=by_rank)]
    all_gather x1, waiting for transfers between devices: 13.1 us -> 16.6 us  [shards(): row_piece = lax.all_gather(hidden, 'tp', axis=0, tiled=True)]
  transfers between devices with their start and end apart: 4 -> 6, of which waited for: 2 -> 4; matrix products, arithmetic and copies ran while one was open for 8% -> 8% of each run, Pallas kernels for 0% -> 0%
where the time goes in v1:
time: 172 us
  matrix products  53.7 us (31%)
  waiting for transfers between devices  52.2 us (30%)
  blocking collectives  19.1 us (11%)
  other arithmetic  14.8 us (9%)
  between operations  13.7 us (8%)
  starting transfers between devices  11.1 us (6%)
  local copies, waits for them, and re-layouts  7.18 us (4%)
    reduce_scatter x1, waiting for transfers between devices, shards(): lax.psum_scatter(jnp.dot(mixed, w_out, preferred_element_type=jnp.float32...  31.8 us
    all_gather x1, waiting for transfers between devices, shards(): row_piece = lax.all_gather(hidden, 'tp', axis=0, tiled=True)  16.6 us
    dot_general x1, matrix products, shards(): jnp.dot(mixed, w_out, preferred_element_type=jnp.float32)  14.5 us
    all_gather x1, blocking collectives, shards(): ctx_all = lax.all_gather(ctx_pair, 'sp', axis=0, tiled=True)  14.3 us
    dot_general x1, matrix products, attend(): jnp.einsum('kgqs,skd->qkgd', near_weights, v_heads, preferred_element_typ...  11 us
    dot_general x1, matrix products, shards(): jnp.dot(row_piece, w_query, preferred_element_type=jnp.float32)  7.75 us
    ppermute x2, starting transfers between devices, perform_modes(): lax.ppermute(spare, group_axis, perm=by_rank)  6.22 us
    dot_general x1, matrix products, attend(): jnp.einsum('kgqs,skd->qkgd', ctx_weights, cv_heads, preferred_element_typ...  5.69 us
  transfers between devices with their start and end apart: 6, of which 4 were waited for; matrix products, arithmetic and copies ran while one was open for 8% of the time, Pallas kernels for 0%

profile of v1, /device:TPU:0, one launch (start us, length us, event | category | flops | bytes accessed | tf_op | source)
XLA Modules:
  0.0 171.9 jit_solution(6107371977890991749)
XLA Ops:
  6.5 0.0 all-gather.2.cloned.1.call-start
  6.5 0.9 multiply_convert_fusion.1
  7.5 0.7 copy-done
  8.2 0.4 fusion.30
  8.6 0.3 copy-done.5
  8.9 0.4 fusion.31
  9.3 0.7 copy-done.6
  10.1 0.4 fusion.38
  10.5 0.0 copy-start.7
  10.5 0.0 copy-start.8
  10.5 3.1 %collective-permute-start = (f32[5,1536]{1,0:T(8,128)S(1)}, f32[5,1536]{1,0:T(8,128)S(1)}, u32[]{:S(2)}, u32[]{:S(2)}) collective-permute-start(f32[5,1536]{1,0:T(8,128)S(1)} %pad_maximum_fusion.5), channel_id=1, source_target_pairs={{0,8},{8,0},{16,24},{24,16},{1,9},{9,1},{17,25},{25,17},{2,10},{10... | collective-permute-start | bytes 92168 | tf_op jit(solution)/shard_map/ppermute | solution.py:148
  13.7 0.0 copy-done.4
  13.7 0.3 fusion.6
  14.0 1.7 %collective-permute-done = f32[5,1536]{1,0:T(8,128)S(1)} collective-permute-done((f32[5,1536]{1,0:T(8,128)S(1)}, f32[5,1536]{1,0:T(8,128)S(1)}, u32[]{:S(2)}, u32[]{:S(2)}) %collective-permute-start) | collective-permute-done | bytes 30752 | tf_op jit(solution)/shard_map/ppermute | solution.py:148
  15.8 3.1 %collective-permute-start.1 = (f32[5,1536]{1,0:T(8,128)S(1)}, f32[5,1536]{1,0:T(8,128)S(1)}, u32[]{:S(2)}, u32[]{:S(2)}) collective-permute-start(f32[5,1536]{1,0:T(8,128)S(1)} %fusion.32), channel_id=1, source_target_pairs={{0,16},{8,24},{16,0},{24,8},{1,17},{9,25},{17,1},{25,9},{2,18},{10... | collective-permute-start | bytes 92168 | tf_op jit(solution)/shard_map/ppermute | solution.py:148
  18.9 2.1 %collective-permute-done.1 = f32[5,1536]{1,0:T(8,128)S(1)} collective-permute-done((f32[5,1536]{1,0:T(8,128)S(1)}, f32[5,1536]{1,0:T(8,128)S(1)}, u32[]{:S(2)}, u32[]{:S(2)}) %collective-permute-start.1) | collective-permute-done | bytes 30752 | tf_op jit(solution)/shard_map/ppermute | solution.py:148
  20.9 4.8 %all_gather.9 = f32[5,3072]{1,0:T(8,128)S(1)} all-gather(f32[5,1536]{1,0:T(8,128)S(1)} %add.157), channel_id=1, replica_groups=mesh['sp'=4,'tp'=2,'dp'=4] {'tp'}, dimensions={1}, use_global_device_ids=true | all-gather | bytes 92160 | tf_op jit(solution)/shard_map/all_gather | solution.py:153
  25.7 0.1 fusion.37
  25.7 0.0 copy-done.10
  25.8 1.4 fusion.10
  27.1 0.0 all-gather.2.cloned.1.call-update
  27.1 0.0 reduce-scatter.2.cloned.1.call-start
  27.2 0.0 copy-done.12
  27.2 0.1 max.30
  27.3 0.1 broadcast_multiply_fusion.1
  27.4 0.2 fusion.21
  27.6 0.2 fusion.15
  27.8 0.3 fusion.14
  28.1 0.4 convolution_convert_fusion.4
  28.5 0.2 copy-done.9
  28.7 0.4 convolution_convert_fusion.3
  29.1 14.3 %all_gather.11 = bf16[128,512]{1,0:T(8,128)(2,1)S(1)} all-gather(bf16[32,512]{1,0:T(8,128)(2,1)S(1)} %pad_maximum_fusion.7), channel_id=1, replica_groups=mesh['sp'=4,'tp'=2,'dp'=4] {'sp'}, dimensions={0}, use_global_device_ids=true | all-gather | bytes 163840 | tf_op jit(solution)/shard_map/all_gather | solution.py:174
  43.5 0.1 copy.26
  43.6 0.7 copy.27
  44.3 16.6 %all-gather.2.cloned.1.call-done = bf16[320,3072]{1,0:T(8,128)(2,1)} async-done(((bf16[160,3072]{1,0:T(8,128)(2,1)}), bf16[320,3072]{1,0:T(8,128)(2,1)}) %all-gather.2.cloned.1.call-update) | async-done | bytes 1966096 | tf_op jit(solution)/shard_map/all_gather | solution.py:175
  60.9 2.6 %fusion.39 = f32[320,256]{0,1:T(8,128)S(1)} fusion(bf16[320,3072]{1,0:T(8,128)(2,1)} %all-gather.2.cloned.1.call-done, bf16[3072,256]{1,0:T(8,128)(2,1)S(1)} %copy-done.8), kind=kOutput, calls=%fused_computation.88 | convolution fusion | flops 503316480 | bytes 3866624 | tf_op jit(solution)/shard_map/dot_general | solution.py:179
  63.5 0.1 subtract_convert_fusion.1
  63.6 0.1 copy.22
  63.8 2.8 %convolution_convert_fusion.2 = bf16[320,256]{1,0:T(8,128)(2,1)S(1)} fusion(bf16[320,3072]{1,0:T(8,128)(2,1)} %all-gather.2.cloned.1.call-done, bf16[3072,256]{1,0:T(8,128)(2,1)} %param.24), kind=kOutput, calls=%fused_computation.29 | convolution fusion | flops 503398400 | bytes 3702784 | tf_op jit(solution)/shard_map/dot_general | solution.py:180
  66.6 3.4 %collective-permute-start.2 = (bf16[128,512]{1,0:T(8,128)(2,1)S(1)}, bf16[128,512]{1,0:T(8,128)(2,1)S(1)}, u32[]{:S(2)}, u32[]{:S(2)}) collective-permute-start(bf16[128,512]{1,0:T(8,128)(2,1)S(1)} %get-tuple-element.11), channel_id=1, source_target_pairs={{0,8},{8,16},{16,24},{1,9},{9,17},{17,25},{2,10},{10,18},{18,26},{... | collective-permute-start | bytes 393224 | tf_op jit(solution)/shard_map/ppermute | solution.py:19
  70.0 1.5 collective-permute-start.3
  71.5 0.0 copy-done.13
  71.5 7.7 %fusion.40 = f32[320,1536]{0,1:T(8,128)S(1)} fusion(bf16[320,3072]{1,0:T(8,128)(2,1)S(1)} %copy-done.13, bf16[3072,1536]{1,0:T(8,128)(2,1)} %param.22), kind=kOutput, calls=%fused_computation.89 | convolution fusion | flops 3019898880 | bytes 13369344 | tf_op jit(solution)/shard_map/dot_general | solution.py:178
  79.3 0.4 subtract_convert_fusion
  79.6 0.2 pad_maximum_fusion
  79.8 2.8 %bitcast_reduce_fusion = (f32[4,6,320]{2,1,0:T(8,128)S(1)}, f32[4,128,320,6]{1,2,3,0:T(8,128)}) fusion(bf16[128,4,64,1]{0,2,3,1:T(8,128)(2,1)S(1)} %bitcast.91, bf16[320,4,6,64]{0,3,2,1:T(8,128)(2,1)S(1)} %bitcast.83), kind=kOutput, calls=%fused_computation.8 | convolution fusion | flops 127787520 | bytes 5011456 | tf_op jit(solution)/shard_map/qkgd,skd->kgqs/dot_general | solution.py:79
  82.6 0.0 collective-permute-done.2
  82.6 0.0 collective-permute-done.3
  82.7 0.8 fusion.35
  83.4 1.2 copy.24
  84.6 4.5 %fusion.1 = (f32[4,6,320]{2,1,0:T(8,128)S(1)}, f32[4,576,320,6]{1,2,3,0:T(8,128)S(1)}) fusion(pred[320,576]{1,0:T(8,128)(4,1)S(1)} %fusion.14, bf16[576,4,64,1]{0,2,3,1:T(8,128)(2,1)S(1)} %bitcast.87, bf16[320,4,6,64]{0,3,2,1:T(8,128)(2,1)S(1)} %bitcast.84), kind=kOutput, calls=%fused_computation.4 | convolution fusion | flops 579494400 | bytes 19187712 | tf_op jit(solution)/shard_map/qkgd,skd->kgqs/dot_general | solution.py:70
  89.1 0.1 maximum_maximum_fusion
  89.2 2.6 %fusion.4 = f32[4,6,320]{2,1,0:T(8,128)S(1)} fusion(f32[4,128,320,6]{1,2,3,0:T(8,128)S(1)} %copy-done.3, f32[4,6,320]{2,1,0:T(8,128)S(1)} %maximum_maximum_fusion), kind=kLoop, calls=%fused_computation.11 | loop fusion | flops 2941440 | bytes 3993600 | tf_op jit(solution)/shard_map/reduce_sum | solution.py:93
  91.8 5.5 %fusion = f32[4,6,320]{2,1,0:T(8,128)S(1)} fusion(f32[4,576,320,6]{1,2,3,0:T(8,128)S(1)} %get-tuple-element.25, f32[4,6,320]{2,1,0:T(8,128)S(1)} %maximum_maximum_fusion, pred[320,576]{1,0:T(8,128)(4,1)S(1)} %fusion.14), kind=kLoop, calls=%fused_computation.3 | loop fusion | flops 17687040 | bytes 17940480 | tf_op jit(solution)/shard_map/reduce_sum | solution.py:92
  97.3 0.0 copy-done.2
  97.3 0.2 copy.23
  97.5 0.1 exponential_add_fusion
  97.6 5.7 %fusion.12 = f32[4,64,6,320]{3,1,2,0:T(8,128)S(1)} fusion(bf16[128,4,64,1]{0,2,3,1:T(8,128)(2,1)S(1)} %bitcast.96, f32[4,128,320,6]{1,2,3,0:T(8,128)} %get-tuple-element.27, f32[4,6,320]{2,1,0:T(8,128)S(1)} %exponential_add_fusion, f32[4,6,320]{2,1,0:T(8,128)S(1)} %maximum_maximum_fusion), kind=kOutput, calls=%fused_computation.24 | convolution fusion | flops 129761280 | bytes 6025216 | tf_op jit(solution)/shard_map/kgqs,skd->qkgd/dot_general | solution.py:99
  103.3 11.0 %fusion.13 = f32[4,64,6,320]{3,1,2,0:T(8,128)} fusion(f32[4,64,6,320]{3,1,2,0:T(8,128)S(1)} %fusion.12, bf16[576,4,64,1]{0,2,3,1:T(8,128)(2,1)S(1)} %bitcast.90, f32[4,576,320,6]{1,2,3,0:T(8,128)} %copy-done.2, f32[4,6,320]{2,1,0:T(8,128)S(1)} %exponential_add_fusion, f32[4,6,320]{2,1,0:T(8,128)S(1)} %maximum_maximum_fusion, pred[320,576]{1,0:T(8,128)(4,1)S(1)} %fusion.14), kind=kOutput, calls=%fused_computation.25 | convolution fusion | flops 588840960 | bytes 22167552 | tf_op jit(solution)/shard_map/kgqs,skd->qkgd/dot_general | solution.py:98
  114.2 2.0 %copy.28 = f32[320,1536]{1,0:T(8,128)S(1)} copy(f32[320,1536]{0,1:T(8,128)} %bitcast.85) | data formatting | bytes 3932160 | tf_op jit(solution)/shard_map/reshape | solution.py:102
  116.2 14.5 %convolution_convert_fusion = bf16[320,3072]{1,0:T(8,128)(2,1)} fusion(bf16[1536,3072]{1,0:T(8,128)(2,1)} %param.26, f32[320,1536]{1,0:T(8,128)S(1)} %copy.28, bf16[320,3072]{1,0:T(8,128)(2,1)} %all-gather.2.cloned.1.call-done, bf16[3072,1536]{1,0:T(8,128)(2,1)} %param.25), kind=kOutput, calls=%fused_computation.6 | convolution fusion | flops 6044712960 | bytes 24772608 | tf_op jit(solution)/shard_map/dot_general | solution.py:207
  130.8 0.0 reduce-scatter.2.cloned.1.call-update
  130.8 31.8 %reduce-scatter.2.cloned.1.call-done = bf16[160,3072]{1,0:T(8,128)(2,1)} async-done(((bf16[320,3072]{1,0:T(8,128)(2,1)}), bf16[160,3072]{1,0:T(8,128)(2,1)}) %reduce-scatter.2.cloned.1.call-update) | async-done | bytes 983056 | tf_op jit(solution)/shard_map/reduce_scatter | solution.py:206
  162.6 2.5 %fusion.11 = bf16[160,3072]{1,0:T(8,128)(2,1)} fusion(bf16[160,3072]{1,0:T(8,128)(2,1)S(1)} %copy-done.4, bf16[160,3072]{1,0:T(8,128)(2,1)} %reduce-scatter.2.cloned.1.call-done, f32[3072]{0:T(1024)S(1)} %bitcast.97), kind=kLoop, calls=%fused_computation.22 | loop fusion | flops 2457600 | bytes 2961408 | tf_op jit(solution)/shard_map/convert_element_type | solution.py:212
  (35 shorter events, 0.3 us)
Async XLA Ops:
  6.5 1.7 copy-start
  6.5 54.4 %all-gather.2.cloned.1.call-start = ((), (), s32[]{:S(2)}) async-start(), calls=%async_computation.1 | async-start | bytes 2949120 | tf_op jit(solution)/shard_map/all_gather | solution.py:175
  6.5 2.4 %copy-start.5 = (bf16[768,1536]{1,0:T(8,128)(2,1)S(1)}, bf16[768,1536]{1,0:T(8,128)(2,1)}, u32[]{:S(2)}) copy-start(bf16[768,1536]{1,0:T(8,128)(2,1)} %param.18) | copy-start | bytes 7077892
  8.2 1.8 %copy-start.6 = (bf16[768,1536]{1,0:T(8,128)(2,1)S(1)}, bf16[768,1536]{1,0:T(8,128)(2,1)}, u32[]{:S(2)}) copy-start(bf16[768,1536]{1,0:T(8,128)(2,1)} %param.20) | copy-start | bytes 7077892
  8.9 4.7 %copy-start.4 = (bf16[160,3072]{1,0:T(8,128)(2,1)S(1)}, bf16[160,3072]{1,0:T(8,128)(2,1)}, u32[]{:S(2)}) copy-start(bf16[160,3072]{1,0:T(8,128)(2,1)} %param.14) | copy-start | bytes 2949124
  10.1 15.7 %copy-start.10 = (f32[3072]{0:T(1024)S(1)}, f32[3072]{0:T(1024)}, u32[]{:S(2)}) copy-start(f32[3072]{0:T(1024)} %param.21) | copy-start | bytes 36868
  10.5 16.7 %copy-start.12 = (f32[24]{0:T(128)S(1)}, f32[24]{0:T(128)}, u32[]{:S(2)}) copy-start(f32[24]{0:T(128)} %param.27) | copy-start | bytes 292
  10.5 17.1 %copy-start.7 = (bf16[32,3072]{1,0:T(8,128)(2,1)S(1)}, bf16[32,3072]{1,0:T(8,128)(2,1)}, u32[]{:S(2)}) copy-start(bf16[32,3072]{1,0:T(8,128)(2,1)} %param.17) | copy-start | bytes 589828
  10.5 17.5 %copy-start.8 = (bf16[3072,256]{1,0:T(8,128)(2,1)S(1)}, bf16[3072,256]{1,0:T(8,128)(2,1)}, u32[]{:S(2)}) copy-start(bf16[3072,256]{1,0:T(8,128)(2,1)} %param.23) | copy-start | bytes 4718596
  10.5 5.2 %collective-permute-start = (f32[5,1536]{1,0:T(8,128)S(1)}, f32[5,1536]{1,0:T(8,128)S(1)}, u32[]{:S(2)}, u32[]{:S(2)}) collective-permute-start(f32[5,1536]{1,0:T(8,128)S(1)} %pad_maximum_fusion.5), channel_id=1, source_target_pairs={{0,8},{8,0},{16,24},{24,16},{1,9},{9,1},{17,25},{25,17},{2,10},{10... | collective-permute-start | bytes 92168 | tf_op jit(solution)/shard_map/ppermute | solution.py:148
  15.8 5.2 %collective-permute-start.1 = (f32[5,1536]{1,0:T(8,128)S(1)}, f32[5,1536]{1,0:T(8,128)S(1)}, u32[]{:S(2)}, u32[]{:S(2)}) collective-permute-start(f32[5,1536]{1,0:T(8,128)S(1)} %fusion.32), channel_id=1, source_target_pairs={{0,16},{8,24},{16,0},{24,8},{1,17},{9,25},{17,1},{25,9},{2,18},{10... | collective-permute-start | bytes 92168 | tf_op jit(solution)/shard_map/ppermute | solution.py:148
  27.1 135.4 %reduce-scatter.2.cloned.1.call-start = ((), (), s32[]{:S(2)}) async-start(), calls=%async_computation.2 | async-start | bytes 2949120 | tf_op jit(solution)/shard_map/reduce_scatter | solution.py:206
  27.3 1.4 copy-start.9
  63.7 7.7 %copy-start.13 = (bf16[320,3072]{1,0:T(8,128)(2,1)S(1)}, bf16[320,3072]{1,0:T(8,128)(2,1)}, u32[]{:S(2)}) copy-start(bf16[320,3072]{1,0:T(8,128)(2,1)} %all-gather.2.cloned.1.call-done) | copy-start | bytes 5898244
  66.6 16.0 %collective-permute-start.2 = (bf16[128,512]{1,0:T(8,128)(2,1)S(1)}, bf16[128,512]{1,0:T(8,128)(2,1)S(1)}, u32[]{:S(2)}, u32[]{:S(2)}) collective-permute-start(bf16[128,512]{1,0:T(8,128)(2,1)S(1)} %get-tuple-element.11), channel_id=1, source_target_pairs={{0,8},{8,16},{16,24},{1,9},{9,17},{17,25},{2,10},{10,18},{18,26},{... | collective-permute-start | bytes 393224 | tf_op jit(solution)/shard_map/ppermute | solution.py:19
  70.0 12.6 %collective-permute-start.3 = (bf16[128,512]{1,0:T(8,128)(2,1)S(1)}, bf16[128,512]{1,0:T(8,128)(2,1)S(1)}, u32[]{:S(2)}, u32[]{:S(2)}) collective-permute-start(bf16[128,512]{1,0:T(8,128)(2,1)S(1)} %get-tuple-element.12), channel_id=1, source_target_pairs={{8,0},{16,8},{24,16},{9,1},{17,9},{25,17},{10,2},{18,10},{26,18},{... | collective-permute-start | bytes 393224 | tf_op jit(solution)/shard_map/ppermute | solution.py:22
  84.6 4.6 %copy-start.3 = (f32[4,128,320,6]{1,2,3,0:T(8,128)S(1)}, f32[4,128,320,6]{1,2,3,0:T(8,128)}, u32[]{:S(2)}) copy-start(f32[4,128,320,6]{1,2,3,0:T(8,128)} %get-tuple-element.27) | copy-start | bytes 11796484
  89.1 8.1 %copy-start.2 = (f32[4,576,320,6]{1,2,3,0:T(8,128)}, f32[4,576,320,6]{1,2,3,0:T(8,128)S(1)}, u32[]{:S(2)}) copy-start(f32[4,576,320,6]{1,2,3,0:T(8,128)S(1)} %get-tuple-element.25) | copy-start | bytes 53084164
  91.8 5.8 %copy-start.11 = (bf16[128,256]{0,1:T(8,128)(2,1)S(1)}, bf16[128,256]{0,1:T(8,128)(2,1)}, u32[]{:S(2)}) copy-start(bf16[128,256]{0,1:T(8,128)(2,1)} %copy.27) | copy-start | bytes 196612
  130.8 34.3 %copy-start.1 = (bf16[768,1536]{1,0:T(8,128)(2,1)S(1)}, bf16[768,1536]{1,0:T(8,128)(2,1)}, u32[]{:S(2)}) copy-start(bf16[768,1536]{1,0:T(8,128)(2,1)} %param.19) | copy-start | bytes 7077892
Sparse Core Ops, SparseCore 0:
  27.3 33.5 all-gather.1
  130.9 31.6 reduce-scatter.1
